TPU v7x, 512 devices: a whole 4x8x8 slice. The times are simulated.
512 devices in a mesh: sp: 32 (over z, x), tp: 16 (over y, core).
Axes of the slice: x: 4, y: 8, z: 8, core: 2. Of those that a mesh axis runs over, the one named last changes fastest.
Arguments:
- glu_value: bfloat16 [1024, 8192], P('tp', 'sp')
- glu_gate: bfloat16 [1024, 8192], P('tp', 'sp'), may hold values from -8 to 8
- conv_taps: float32 [1024, 31], P('tp'), may hold values from -1 to 1
- norm_gain: float32 [1024], P('tp'), may hold values from 0.1 to 1.9
- out_proj: bfloat16 [1024, 2048], P(None, 'tp'), may hold values from -0.1875 to 0.1875
- resid: bfloat16 [8192, 2048], P('sp', 'tp'), may hold values from -6 to 6
- expert_ids: int32 [8192, 2], P('sp'), may hold values from 0 to 31, all different within a row; in each aligned block of 256 rows (0 to 255, 256 to 511, ...) at most 32 rows name the same one
- route_logits: float32 [8192, 2], P('sp'), may hold values from -8 to 8
- group_prob: float32 [8192], P('sp'), may hold values from 0.2 to 1
- w_gate: bfloat16 [32, 2048, 4096], P('sp', None, 'tp'), may hold values from -0.125 to 0.125
- w_up: bfloat16 [32, 2048, 4096], P('sp', None, 'tp'), may hold values from -0.125 to 0.125
- w_down: bfloat16 [32, 4096, 2048], P('sp', None, 'tp'), may hold values from -0.09375 to 0.09375
Outputs:
- layer_out: bfloat16 [8192, 2048], P('sp', 'tp')
Inputs may be any that keep to these rules, and one draw needn't show every extreme that they name: `expert_ids`: each row names 2 different experts. In each aligned block of 256 rows (the rows of one index of sp) no expert is named by more than 32 rows, a bound that some block reaches.
All inputs are finite; a program needn't handle non-finite values.
Results may differ from a plain program's by a relative error of at most 0.0061.
Values may be sent and summed in bfloat16 or wider, within the bound.
A program may use at most 64 MiB of HBM per device.

v0:
```python
import jax
import jax.numpy as jnp
from jax import lax
from jax.sharding import PartitionSpec as P


def from_behind(block, axis, distance):
    devices = range(lax.axis_size(axis))
    route = [(i - distance, i) for i in devices if i - distance in devices]
    return lax.ppermute(block, axis, route)


def from_everyone(shard, axis):
    copies = jnp.broadcast_to(shard, (lax.axis_size(axis), *shard.shape))
    return lax.all_to_all(copies, axis, split_axis=0, concat_axis=0, tiled=True)


def of_everyone(shard, axis):
    everything = from_everyone(shard, axis)
    return jnp.sum(everything, axis=0)


def packed_total(arrays, axis):
    ends = [0]
    for a in arrays:
        ends.append(ends[-1] + a.size)
    subtotal = of_everyone(jnp.concatenate([a.ravel() for a in arrays]), axis)
    return tuple((subtotal[b:e].reshape(a.shape) for a, b, e in zip(arrays, ends, ends[1:])))


def per_device(
    glu_value,
    glu_gate,
    conv_taps,
    norm_gain,
    out_proj,
    resid,
    expert_ids,
    route_logits,
    group_prob,
    w_gate,
    w_up,
    w_down,
):
    local_tokens = glu_value.shape[1]
    tap_count = conv_taps.shape[1]
    channels = glu_value.shape[0] * lax.axis_size("tp")
    gated = (glu_value.astype(jnp.float32) * jax.nn.sigmoid(glu_gate.astype(jnp.float32))).astype(
        jnp.bfloat16
    )
    history = from_behind(gated[:, local_tokens - (tap_count - 1) :], "sp", 1)
    padded = jnp.concatenate([history, gated], axis=1).astype(jnp.float32)
    filtered = jnp.zeros(gated.shape, jnp.float32)
    for offset in range(tap_count):
        filtered = (
            filtered + conv_taps[:, offset : offset + 1] * padded[:, offset : offset + local_tokens]
        )
    total_one, total_two = packed_total(
        (jnp.sum(filtered, axis=0), jnp.sum(filtered * filtered, axis=0)), "tp"
    )
    mean = total_one / channels
    var = total_two / channels - mean * mean
    normed = (filtered - mean[None, :]) * lax.rsqrt(var[None, :] + 1e-05) * norm_gain[:, None]
    activated = jax.nn.silu(normed).astype(jnp.bfloat16)
    weights = out_proj
    projected = lax.dot_general(
        lax.all_gather(activated, "tp", axis=0, tiled=True),
        weights,
        (((0,), (0,)), ((), ())),
        preferred_element_type=jnp.float32,
    )
    mixed = (resid.astype(jnp.float32) + projected).astype(jnp.bfloat16)
    experts = lax.axis_size("sp")
    capacity = 4 * local_tokens // experts
    flat_ids = expert_ids.reshape(-1)
    onehot = (flat_ids[:, None] == jnp.arange(experts, dtype=jnp.int32)[None, :]).astype(jnp.int32)
    rank = jnp.sum(jnp.cumsum(onehot, axis=0) * onehot, axis=1) - 1
    slot = flat_ids * capacity + rank
    token_of = jnp.arange(flat_ids.shape[0], dtype=jnp.int32) // expert_ids.shape[1]
    table = jnp.zeros((experts * capacity,), jnp.int32).at[slot].set(token_of)
    filled = jnp.zeros((experts * capacity,), jnp.bool_).at[slot].set(True)
    route_weight = (group_prob[:, None] * jax.nn.softmax(route_logits, axis=-1)).reshape(-1)
    outgoing = jnp.where(
        filled[:, None], jnp.take(mixed, table, axis=0), jnp.zeros((), jnp.bfloat16)
    )
    outgoing = outgoing.reshape(experts, capacity, mixed.shape[1])
    rows = lax.all_gather(
        lax.all_to_all(outgoing, "sp", split_axis=0, concat_axis=0, tiled=True),
        "tp",
        axis=2,
        tiled=True,
    )
    sources, count, width = rows.shape
    flat_rows = rows.reshape(sources * count, width)
    gate_part = jnp.dot(flat_rows, w_gate[0], preferred_element_type=jnp.float32)
    up_part = jnp.dot(flat_rows, w_up[0], preferred_element_type=jnp.float32)
    hidden = (jax.nn.silu(gate_part) * up_part).astype(jnp.bfloat16)
    weights = w_down[0]
    expert_out = jnp.dot(
        lax.all_gather(hidden, "tp", axis=1, tiled=True),
        weights,
        preferred_element_type=jnp.float32,
    )
    results = expert_out.astype(jnp.bfloat16).reshape(sources, count, w_down.shape[2])
    returned = lax.all_to_all(results, "sp", split_axis=0, concat_axis=0, tiled=True)
    flat_back = returned.reshape(experts * capacity, returned.shape[2])
    picked = jnp.take(flat_back, slot, axis=0).astype(jnp.float32) * route_weight[:, None]
    routed = jnp.sum(picked.reshape(local_tokens, expert_ids.shape[1], flat_back.shape[1]), axis=1)
    return (mixed.astype(jnp.float32) + routed).astype(jnp.bfloat16)


def solution(mesh):
    return jax.shard_map(
        per_device,
        mesh=mesh,
        in_specs=(
            P("tp", "sp"),
            P("tp", "sp"),
            P("tp", None),
            P("tp"),
            P(None, "tp"),
            P("sp", "tp"),
            P("sp", None),
            P("sp", None),
            P("sp"),
            P("sp", None, "tp"),
            P("sp", None, "tp"),
            P("sp", None, "tp"),
        ),
        out_specs=P("sp", "tp"),
        check_vma=False,
    )
```

profile of v0, /device:TPU:8, one launch (start us, length us, event | category | flops | bytes accessed | tf_op | source)
XLA Modules:
  0.0 238.1 jit_solution(12596920624349899466)
XLA Ops:
  6.5 0.9 multiply_convert_fusion.1
  7.5 0.1 slice.272
  7.5 3.4 %collective-permute-start = (bf16[64,30]{1,0:T(8,128)(2,1)S(1)}, bf16[64,30]{1,0:T(8,128)(2,1)S(1)}, u32[]{:S(2)}, u32[]{:S(2)}) collective-permute-start(bf16[64,30]{1,0:T(8,128)(2,1)S(1)} %slice.272), channel_id=1, source_target_pairs={{0,16},{16,32},{32,48},{48,64},{64,80},{80,96},{96,112},{112,128},... | collective-permute-start | bytes 11528 | tf_op jit(solution)/shard_map/ppermute | solution.py:10
  10.9 1.0 slice_bitcast_fusion.30
  11.9 1.0 slice_bitcast_fusion.29
  12.9 0.8 copy.32
  13.7 0.1 eq.26
  13.9 0.1 reshape.114
  14.0 0.7 broadcast_multiply_fusion
  14.7 1.2 reduce-window.6
  15.9 0.2 slice_reduce_fusion
  16.1 0.1 fusion.7
  16.3 0.1 copy.37
  16.4 0.1 mul.489
  16.6 2.4 %scatter_custom_fusion.1 = s32[1024]{0:T(1024)S(1)} fusion(s32[512]{0:T(512)S(1)} %bitcast.102, s32[512]{0:T(512)S(1)} %add_select_fusion, s32[]{:T(128)} %constant.68.clone.1), kind=kCustom, calls=%fused_computation.106 | custom fusion | bytes 4100 | tf_op jit(solution)/shard_map/scatter | solution.py:80
  19.0 0.1 maximum_convert_fusion
  19.1 0.9 fusion.48
  20.0 0.6 broadcast_in_dim.60
  20.7 7.6 %all-to-all-start = ((f32[16,1,512]{2,1,0:T(1,128)}), f32[16,1,512]{2,1,0:T(1,128)S(1)}, u32[]{:S(2)}, u32[]{:S(2)}) async-start(f32[16,1,512]{2,1,0:T(1,128)} %broadcast_in_dim.60), calls=%async_computation | async-start | bytes 65536 | tf_op jit(solution)/shard_map/all_to_all | solution.py:15
  28.2 0.0 all-gather.3.cloned.1.call-start
  28.3 0.1 broadcast_in_dim.67
  28.4 2.4 %scatter_custom_fusion = pred[1024]{0:T(1024)(128)(4,1)S(1)} fusion(s32[512]{0:T(512)S(1)} %bitcast.103, pred[512]{0:T(512)(128)(4,1)S(1)} %broadcast.121, pred[]{:T(512)} %constant.72.clone.1), kind=kCustom, calls=%fused_computation.109 | custom fusion | bytes 1025 | tf_op jit(solution)/shard_map/scatter | solution.py:81
  30.8 0.1 broadcast_in_dim.64
  30.9 3.6 %all-to-all-done = f32[16,1,512]{2,1,0:T(1,128)S(1)} async-done(((f32[16,1,512]{2,1,0:T(1,128)}), f32[16,1,512]{2,1,0:T(1,128)S(1)}, u32[]{:S(2)}, u32[]{:S(2)}) %all-to-all-start) | async-done | bytes 32800 | tf_op jit(solution)/shard_map/all_to_all | solution.py:15
  34.6 0.8 multiply_convert_fusion
  35.3 17.0 %all_gather.9 = bf16[1024,256]{1,0:T(8,128)(2,1)S(1)} all-gather(bf16[64,256]{1,0:T(8,128)(2,1)S(1)} %multiply_convert_fusion), channel_id=1, replica_groups=mesh['sp'=32,'tp'=16] {'tp'}, dimensions={0}, use_global_device_ids=true | all-gather | bytes 557056 | tf_op jit(solution)/shard_map/all_gather | solution.py:67
  52.4 0.3 fusion.1
  52.7 3.2 %gather_fusion = bf16[1024,128]{1,0:T(8,128)(2,1)S(1)} fusion(bf16[256,128]{1,0:T(8,128)(2,1)S(1)} %fusion.1, s32[1024]{0:T(1024)S(1)} %fusion.39), kind=kCustom, calls=%fused_computation | custom fusion | bytes 528384 | tf_op jit(solution)/shard_map/jit(_take)/gather | solution.py:84
  55.9 0.3 select_select_fusion
  56.3 0.0 copy-start.7
  56.3 26.5 %all_to_all.16 = bf16[32,32,128]{2,1,0:T(8,128)(2,1)} all-to-all(bf16[32,32,128]{2,1,0:T(8,128)(2,1)S(1)} %select_select_fusion), channel_id=1, replica_groups=mesh['sp'=32,'tp'=16] {'sp'}, dimensions={0} | all-to-all | bytes 524288 | tf_op jit(solution)/shard_map/all_to_all | solution.py:88
  82.7 0.0 all-gather.3.cloned.1.call-update
  82.8 0.0 all-gather.5.cloned.1.call-start
  82.8 43.3 %all-gather.3.cloned.1.call-done = bf16[32,32,2048]{2,1,0:T(8,128)(2,1)} async-done(((bf16[32,32,128]{2,1,0:T(8,128)(2,1)}), bf16[32,32,2048]{2,1,0:T(8,128)(2,1)}) %all-gather.3.cloned.1.call-update) | async-done | bytes 4194320 | tf_op jit(solution)/shard_map/all_gather | solution.py:87
  126.1 3.6 %fusion.4 = f32[1024,256]{1,0:T(8,128)S(1)} fusion(bf16[1024,2048]{1,0:T(8,128)(2,1)} %bitcast.105, bf16[1,2048,256]{2,1,0:T(8,128)(2,1)S(1)} %copy-done), kind=kOutput, calls=%fused_computation.11 | convolution fusion | flops 1073741824 | bytes 6291456 | tf_op jit(solution)/shard_map/dot_general | solution.py:95
  129.8 2.1 fusion
  131.9 0.0 all-gather.5.cloned.1.call-update
  131.9 0.1 sub.37
  132.1 0.1 copy.35
  132.2 66.1 %all-gather.5.cloned.1.call-done = bf16[1024,4096]{1,0:T(8,128)(2,1)} async-done(((bf16[1024,256]{1,0:T(8,128)(2,1)}), bf16[1024,4096]{1,0:T(8,128)(2,1)}) %all-gather.5.cloned.1.call-update) | async-done | bytes 8388624 | tf_op jit(solution)/shard_map/all_gather | solution.py:100
  198.3 6.6 %convolution_convert_fusion = bf16[1024,128]{1,0:T(8,128)(2,1)} fusion(bf16[1024,4096]{1,0:T(8,128)(2,1)} %all-gather.5.cloned.1.call-done, bf16[1,4096,128]{2,1,0:T(8,128)(2,1)} %param.23), kind=kOutput, calls=%fused_computation.6 | convolution fusion | flops 1073872896 | bytes 9699328 | tf_op jit(solution)/shard_map/dot_general | solution.py:99
  204.9 9.4 %all-to-all-start.2 = ((bf16[32,32,128]{2,1,0:T(8,128)(2,1)}), bf16[32,32,128]{2,1,0:T(8,128)(2,1)S(1)}, u32[]{:S(2)}, u32[]{:S(2)}) async-start(bf16[32,32,128]{2,1,0:T(8,128)(2,1)} %bitcast.39), calls=%async_computation.2 | async-start | bytes 524288 | tf_op jit(solution)/shard_map/all_to_all | solution.py:105
  214.4 0.2 copy.36
  214.6 0.1 copy.38
  214.8 13.0 %all-to-all-done.2 = bf16[32,32,128]{2,1,0:T(8,128)(2,1)S(1)} async-done(((bf16[32,32,128]{2,1,0:T(8,128)(2,1)}), bf16[32,32,128]{2,1,0:T(8,128)(2,1)S(1)}, u32[]{:S(2)}, u32[]{:S(2)}) %all-to-all-start.2) | async-done | bytes 262176 | tf_op jit(solution)/shard_map/all_to_all | solution.py:105
  227.8 1.3 gather_fusion.1
  229.1 1.5 multiply_reduce_fusion
  230.6 0.7 add_convert_fusion
  (33 shorter events, 0.3 us)
Async XLA Ops:
  6.5 119.6 %copy-start = (bf16[1,2048,256]{2,1,0:T(8,128)(2,1)S(1)}, bf16[1,2048,256]{2,1,0:T(8,128)(2,1)}, u32[]{:S(2)}) copy-start(bf16[1,2048,256]{2,1,0:T(8,128)(2,1)} %param.21) | copy-start | bytes 3145732
  6.5 45.8 %copy-start.1 = (bf16[1024,128]{1,0:T(8,128)(2,1)S(1)}, bf16[1024,128]{1,0:T(8,128)(2,1)}, u32[]{:S(2)}) copy-start(bf16[1024,128]{1,0:T(8,128)(2,1)} %param.16) | copy-start | bytes 786436
  6.5 45.8 %copy-start.2 = (bf16[256,128]{1,0:T(8,128)(2,1)S(1)}, bf16[256,128]{1,0:T(8,128)(2,1)}, u32[]{:S(2)}) copy-start(bf16[256,128]{1,0:T(8,128)(2,1)} %param.17) | copy-start | bytes 196612
  7.5 11.5 %collective-permute-start = (bf16[64,30]{1,0:T(8,128)(2,1)S(1)}, bf16[64,30]{1,0:T(8,128)(2,1)S(1)}, u32[]{:S(2)}, u32[]{:S(2)}) collective-permute-start(bf16[64,30]{1,0:T(8,128)(2,1)S(1)} %slice.272), channel_id=1, source_target_pairs={{0,16},{16,32},{32,48},{48,64},{64,80},{80,96},{96,112},{112,128},... | collective-permute-start | bytes 11528 | tf_op jit(solution)/shard_map/ppermute | solution.py:10
  20.7 13.9 %all-to-all-start = ((f32[16,1,512]{2,1,0:T(1,128)}), f32[16,1,512]{2,1,0:T(1,128)S(1)}, u32[]{:S(2)}, u32[]{:S(2)}) async-start(f32[16,1,512]{2,1,0:T(1,128)} %broadcast_in_dim.60), calls=%async_computation | async-start | bytes 65536 | tf_op jit(solution)/shard_map/all_to_all | solution.py:15
  28.2 97.9 %all-gather.3.cloned.1.call-start = ((), (), s32[]{:S(2)}) async-start(), calls=%async_computation.3 | async-start | bytes 4456448 | tf_op jit(solution)/shard_map/all_gather | solution.py:87
  56.3 73.5 %copy-start.7 = (bf16[1,2048,256]{2,1,0:T(8,128)(2,1)S(1)}, bf16[1,2048,256]{2,1,0:T(8,128)(2,1)}, u32[]{:S(2)}) copy-start(bf16[1,2048,256]{2,1,0:T(8,128)(2,1)} %param.22) | copy-start | bytes 3145732
  82.8 115.5 %all-gather.5.cloned.1.call-start = ((), (), s32[]{:S(2)}) async-start(), calls=%async_computation.4 | async-start | bytes 8912896 | tf_op jit(solution)/shard_map/all_gather | solution.py:100
  126.1 3.6 %copy-start.6 = (bf16[32,32,2048]{2,1,0:T(8,128)(2,1)S(1)}, bf16[32,32,2048]{2,1,0:T(8,128)(2,1)}, u32[]{:S(2)}) copy-start(bf16[32,32,2048]{2,1,0:T(8,128)(2,1)} %all-gather.3.cloned.1.call-done) | copy-start | bytes 12582916
  132.2 82.2 %copy-start.3 = (s32[256,2]{0,1:T(2,128)S(1)}, s32[256,2]{0,1:T(2,128)}, u32[]{:S(2)}) copy-start(s32[256,2]{0,1:T(2,128)} %param.18) | copy-start | bytes 6148
  132.2 82.4 %copy-start.4 = (f32[256,2]{0,1:T(2,128)S(1)}, f32[256,2]{0,1:T(2,128)}, u32[]{:S(2)}) copy-start(f32[256,2]{0,1:T(2,128)} %param.19) | copy-start | bytes 6148
  132.2 82.5 %copy-start.5 = (f32[256]{0:T(256)S(1)}, f32[256]{0:T(256)}, u32[]{:S(2)}) copy-start(f32[256]{0:T(256)} %param.20) | copy-start | bytes 3076
  204.9 22.8 %all-to-all-start.2 = ((bf16[32,32,128]{2,1,0:T(8,128)(2,1)}), bf16[32,32,128]{2,1,0:T(8,128)(2,1)S(1)}, u32[]{:S(2)}, u32[]{:S(2)}) async-start(bf16[32,32,128]{2,1,0:T(8,128)(2,1)} %bitcast.39), calls=%async_computation.2 | async-start | bytes 524288 | tf_op jit(solution)/shard_map/all_to_all | solution.py:105
Sparse Core Ops, SparseCore 0:
  82.9 43.2 all-gather.2
  132.1 66.1 all-gather.4
where the time goes:
time: 239 us; the launch traced here: 238 us
  waiting for transfers between devices  126 us (53%)
  blocking collectives  43.5 us (18%)
  starting transfers between devices  20.4 us (9%)
  local copies, waits for them, and re-layouts  14.4 us (6%)
  between operations  13.7 us (6%)
  matrix products  12.7 us (5%)
  other arithmetic  7.23 us (3%)
    all_gather x1, waiting for transfers between devices, per_device(): lax.all_gather(hidden, 'tp', axis=1, tiled=True)  66.1 us
    all_gather x1, waiting for transfers between devices, per_device(): lax.all_gather(lax.all_to_all(outgoing, 'sp', split_axis=0, concat_axis=0...  43.3 us
    all_to_all x1, blocking collectives, per_device(): lax.all_to_all(outgoing, 'sp', split_axis=0, concat_axis=0, tiled=True)  26.5 us
    all_gather x1, blocking collectives, per_device(): lax.all_gather(activated, 'tp', axis=0, tiled=True)  17 us
    all_to_all x1, waiting for transfers between devices, per_device(): lax.all_to_all(results, 'sp', split_axis=0, concat_axis=0, tiled=True)  13 us
    all_to_all x1, starting transfers between devices, per_device(): lax.all_to_all(results, 'sp', split_axis=0, concat_axis=0, tiled=True)  9.41 us
    all_to_all x1, starting transfers between devices, from_everyone(): return lax.all_to_all(copies, axis, split_axis=0, concat_axis=0, tiled=True)  7.56 us
    dot_general x1, matrix products, per_device(): jnp.dot(lax.all_gather(hidden, 'tp', axis=1, tiled=True), weights, prefer...  6.65 us
  transfers between devices with their start and end apart: 5, of which 4 were waited for; matrix products, arithmetic and copies ran while one was open for 5% of the time, Pallas kernels for 0%

commit v1 on v0

--- a/solution.py
+++ b/solution.py
@@ -97,7 +97,9 @@
     hidden = (jax.nn.silu(gate_part) * up_part).astype(jnp.bfloat16)
     weights = w_down[0]
     expert_out = jnp.dot(
-        lax.all_gather(hidden, "tp", axis=1, tiled=True),
+        jnp.concatenate(
+            lax.all_to_all(jnp.stack([hidden] * lax.axis_size("tp")), "tp", 0, 0), axis=1
+        ),
         weights,
         preferred_element_type=jnp.float32,
     )

time: 239 us -> 366 us (1.53)
  the two profiles are of different devices: /device:TPU:8 before, /device:TPU:24 now
where the time goes in v1:
time: 366 us; the launch traced here: 365 us
  waiting for transfers between devices  243 us (66%)
  blocking collectives  43.1 us (12%)
  starting transfers between devices  27.4 us (7%)
  local copies, waits for them, and re-layouts  18.9 us (5%)
  between operations  13.7 us (4%)
  matrix products  11.7 us (3%)
  other arithmetic  7.23 us (2%)
    all_to_all x1, waiting for transfers between devices, per_device(): lax.all_to_all(jnp.stack([hidden] * lax.axis_size('tp')), 'tp', 0, 0)  183 us
    all_gather x1, waiting for transfers between devices, per_device(): lax.all_gather(lax.all_to_all(outgoing, 'sp', split_axis=0, concat_axis=0...  44.7 us
    all_to_all x1, blocking collectives, per_device(): lax.all_to_all(outgoing, 'sp', split_axis=0, concat_axis=0, tiled=True)  26.5 us
    all_gather x1, blocking collectives, per_device(): lax.all_gather(activated, 'tp', axis=0, tiled=True)  16.6 us
    all_to_all x1, waiting for transfers between devices, per_device(): lax.all_to_all(results, 'sp', split_axis=0, concat_axis=0, tiled=True)  12.8 us
    all_to_all x1, starting transfers between devices, per_device(): lax.all_to_all(results, 'sp', split_axis=0, concat_axis=0, tiled=True)  9.23 us
    all_to_all x1, starting transfers between devices, per_device(): lax.all_to_all(jnp.stack([hidden] * lax.axis_size('tp')), 'tp', 0, 0)  7.44 us
    all_to_all x1, starting transfers between devices, from_everyone(): return lax.all_to_all(copies, axis, split_axis=0, concat_axis=0, tiled=True)  7.34 us
  transfers between devices with their start and end apart: 5, of which 4 were waited for; matrix products, arithmetic and copies ran while one was open for 3% of the time, Pallas kernels for 0%

profile of v1, /device:TPU:24, one launch (start us, length us, event | category | flops | bytes accessed | tf_op | source)
XLA Modules:
  0.0 364.9 jit_solution(3360036895538678196)
XLA Ops:
  6.5 0.9 multiply_convert_fusion.1
  7.5 0.1 slice.272
  7.5 3.4 collective-permute-start
  10.9 1.0 slice_bitcast_fusion.30
  11.9 1.0 slice_bitcast_fusion.29
  12.9 0.8 copy.35
  13.7 0.1 eq.26
  13.9 0.1 reshape.122
  14.0 0.7 broadcast_multiply_fusion
  14.7 1.2 reduce-window.6
  15.9 0.2 slice_reduce_fusion
  16.1 0.1 fusion.7
  16.3 0.1 copy.40
  16.4 0.1 mul.489
  16.6 2.4 scatter_custom_fusion.1
  19.0 0.1 maximum_convert_fusion
  19.1 0.9 fusion.48
  20.0 0.6 broadcast_in_dim.60
  20.7 7.3 %all-to-all-start = ((f32[16,1,512]{2,1,0:T(1,128)}), f32[16,1,512]{2,1,0:T(1,128)S(1)}, u32[]{:S(2)}, u32[]{:S(2)}) async-start(f32[16,1,512]{2,1,0:T(1,128)} %broadcast_in_dim.60), calls=%async_computation | async-start | bytes 65536 | tf_op jit(solution)/shard_map/all_to_all | solution.py:15
  28.0 0.0 all-gather.2.cloned.1.call-start
  28.0 0.1 broadcast_in_dim.67
  28.1 2.4 scatter_custom_fusion
  30.6 0.1 broadcast_in_dim.64
  30.7 1.9 all-to-all-done
  32.7 0.8 multiply_convert_fusion
  33.4 16.6 %all_gather.6 = bf16[1024,256]{1,0:T(8,128)(2,1)S(1)} all-gather(bf16[64,256]{1,0:T(8,128)(2,1)S(1)} %multiply_convert_fusion), channel_id=1, replica_groups=mesh['sp'=32,'tp'=16] {'tp'}, dimensions={0}, use_global_device_ids=true | all-gather | bytes 557056 | tf_op jit(solution)/shard_map/all_gather | solution.py:67
  50.0 0.3 fusion.1
  50.4 3.2 gather_fusion
  53.6 0.3 select_select_fusion
  54.0 26.5 %all_to_all.21 = bf16[32,32,128]{2,1,0:T(8,128)(2,1)} all-to-all(bf16[32,32,128]{2,1,0:T(8,128)(2,1)S(1)} %select_select_fusion), channel_id=1, replica_groups=mesh['sp'=32,'tp'=16] {'sp'}, dimensions={0} | all-to-all | bytes 524288 | tf_op jit(solution)/shard_map/all_to_all | solution.py:88
  80.4 0.0 all-gather.2.cloned.1.call-update
  80.4 44.7 %all-gather.2.cloned.1.call-done = bf16[32,32,2048]{2,1,0:T(8,128)(2,1)} async-done(((bf16[32,32,128]{2,1,0:T(8,128)(2,1)}), bf16[32,32,2048]{2,1,0:T(8,128)(2,1)}) %all-gather.2.cloned.1.call-update) | async-done | bytes 4194320 | tf_op jit(solution)/shard_map/all_gather | solution.py:87
  125.2 3.6 fusion.4
  128.8 1.3 fusion
  130.1 0.2 copy.41
  130.3 4.3 %stack.2 = bf16[16,1024,256]{1,2,0:T(8,128)(2,1)} broadcast(bf16[1024,256]{0,1:T(8,128)(2,1)S(1)} %copy.41), dimensions={1,2} | broadcast | bytes 8912896 | tf_op jit(solution)/shard_map/stack | solution.py:101
  134.6 7.4 %all-to-all-start.2 = ((bf16[16,1024,256]{1,2,0:T(8,128)(2,1)}), bf16[16,1024,256]{1,2,0:T(8,128)(2,1)}, u32[]{:S(2)}, u32[]{:S(2)}) async-start(bf16[16,1024,256]{1,2,0:T(8,128)(2,1)} %stack.2), calls=%async_computation.2 | async-start | bytes 16777216 | tf_op jit(solution)/shard_map/all_to_all | solution.py:101
  142.0 0.1 sub.37
  142.2 0.1 copy.38
  142.2 183.4 %all-to-all-done.2 = bf16[16,1024,256]{1,2,0:T(8,128)(2,1)} async-done(((bf16[16,1024,256]{1,2,0:T(8,128)(2,1)}), bf16[16,1024,256]{1,2,0:T(8,128)(2,1)}, u32[]{:S(2)}, u32[]{:S(2)}) %all-to-all-start.2) | async-done | bytes 8388640 | tf_op jit(solution)/shard_map/all_to_all | solution.py:101
  325.6 6.5 %convolution_convert_fusion = bf16[1024,128]{1,0:T(8,128)(2,1)} fusion(bf16[1024,4096]{0,1:T(8,128)(2,1)} %bitcast.39, bf16[1,4096,128]{2,1,0:T(8,128)(2,1)S(1)} %copy-done.8), kind=kOutput, calls=%fused_computation.6 | convolution fusion | flops 1073872896 | bytes 9699328 | tf_op jit(solution)/shard_map/dot_general | solution.py:99
  332.2 9.2 %all-to-all-start.3 = ((bf16[32,32,128]{2,1,0:T(8,128)(2,1)}), bf16[32,32,128]{2,1,0:T(8,128)(2,1)S(1)}, u32[]{:S(2)}, u32[]{:S(2)}) async-start(bf16[32,32,128]{2,1,0:T(8,128)(2,1)} %bitcast.41), calls=%async_computation.3 | async-start | bytes 524288 | tf_op jit(solution)/shard_map/all_to_all | solution.py:107
  341.4 0.2 copy.39
  341.7 0.1 copy.42
  341.9 12.8 %all-to-all-done.3 = bf16[32,32,128]{2,1,0:T(8,128)(2,1)S(1)} async-done(((bf16[32,32,128]{2,1,0:T(8,128)(2,1)}), bf16[32,32,128]{2,1,0:T(8,128)(2,1)S(1)}, u32[]{:S(2)}, u32[]{:S(2)}) %all-to-all-start.3) | async-done | bytes 262176 | tf_op jit(solution)/shard_map/all_to_all | solution.py:107
  354.6 1.3 gather_fusion.1
  356.0 1.5 multiply_reduce_fusion
  357.4 0.6 add_convert_fusion
  (36 shorter events, 0.3 us)
Async XLA Ops:
  6.5 118.6 %copy-start = (bf16[1,2048,256]{2,1,0:T(8,128)(2,1)S(1)}, bf16[1,2048,256]{2,1,0:T(8,128)(2,1)}, u32[]{:S(2)}) copy-start(bf16[1,2048,256]{2,1,0:T(8,128)(2,1)} %param.21) | copy-start | bytes 3145732
  6.5 43.5 %copy-start.1 = (bf16[1024,128]{1,0:T(8,128)(2,1)S(1)}, bf16[1024,128]{1,0:T(8,128)(2,1)}, u32[]{:S(2)}) copy-start(bf16[1024,128]{1,0:T(8,128)(2,1)} %param.16) | copy-start | bytes 786436
  6.5 43.5 %copy-start.2 = (bf16[256,128]{1,0:T(8,128)(2,1)S(1)}, bf16[256,128]{1,0:T(8,128)(2,1)}, u32[]{:S(2)}) copy-start(bf16[256,128]{1,0:T(8,128)(2,1)} %param.17) | copy-start | bytes 196612
  7.5 11.5 %collective-permute-start = (bf16[64,30]{1,0:T(8,128)(2,1)S(1)}, bf16[64,30]{1,0:T(8,128)(2,1)S(1)}, u32[]{:S(2)}, u32[]{:S(2)}) collective-permute-start(bf16[64,30]{1,0:T(8,128)(2,1)S(1)} %slice.272), channel_id=1, source_target_pairs={{0,16},{16,32},{32,48},{48,64},{64,80},{80,96},{96,112},{112,128},... | collective-permute-start | bytes 11528 | tf_op jit(solution)/shard_map/ppermute | solution.py:10
  20.7 12.0 %all-to-all-start = ((f32[16,1,512]{2,1,0:T(1,128)}), f32[16,1,512]{2,1,0:T(1,128)S(1)}, u32[]{:S(2)}, u32[]{:S(2)}) async-start(f32[16,1,512]{2,1,0:T(1,128)} %broadcast_in_dim.60), calls=%async_computation | async-start | bytes 65536 | tf_op jit(solution)/shard_map/all_to_all | solution.py:15
  28.0 97.2 %all-gather.2.cloned.1.call-start = ((), (), s32[]{:S(2)}) async-start(), calls=%async_computation.4 | async-start | bytes 4456448 | tf_op jit(solution)/shard_map/all_gather | solution.py:87
  53.9 74.8 %copy-start.7 = (bf16[1,2048,256]{2,1,0:T(8,128)(2,1)S(1)}, bf16[1,2048,256]{2,1,0:T(8,128)(2,1)}, u32[]{:S(2)}) copy-start(bf16[1,2048,256]{2,1,0:T(8,128)(2,1)} %param.22) | copy-start | bytes 3145732
  125.2 3.6 copy-start.6
  134.6 191.1 %copy-start.8 = (bf16[1,4096,128]{2,1,0:T(8,128)(2,1)S(1)}, bf16[1,4096,128]{2,1,0:T(8,128)(2,1)}, u32[]{:S(2)}) copy-start(bf16[1,4096,128]{2,1,0:T(8,128)(2,1)} %param.23) | copy-start | bytes 3145732
  134.6 191.1 %all-to-all-start.2 = ((bf16[16,1024,256]{1,2,0:T(8,128)(2,1)}), bf16[16,1024,256]{1,2,0:T(8,128)(2,1)}, u32[]{:S(2)}, u32[]{:S(2)}) async-start(bf16[16,1024,256]{1,2,0:T(8,128)(2,1)} %stack.2), calls=%async_computation.2 | async-start | bytes 16777216 | tf_op jit(solution)/shard_map/all_to_all | solution.py:101
  325.6 15.8 %copy-start.3 = (s32[256,2]{0,1:T(2,128)S(1)}, s32[256,2]{0,1:T(2,128)}, u32[]{:S(2)}) copy-start(s32[256,2]{0,1:T(2,128)} %param.18) | copy-start | bytes 6148
  325.6 16.0 %copy-start.4 = (f32[256,2]{0,1:T(2,128)S(1)}, f32[256,2]{0,1:T(2,128)}, u32[]{:S(2)}) copy-start(f32[256,2]{0,1:T(2,128)} %param.19) | copy-start | bytes 6148
  325.6 16.0 %copy-start.5 = (f32[256]{0:T(256)S(1)}, f32[256]{0:T(256)}, u32[]{:S(2)}) copy-start(f32[256]{0:T(256)} %param.20) | copy-start | bytes 3076
  332.2 22.5 %all-to-all-start.3 = ((bf16[32,32,128]{2,1,0:T(8,128)(2,1)}), bf16[32,32,128]{2,1,0:T(8,128)(2,1)S(1)}, u32[]{:S(2)}, u32[]{:S(2)}) async-start(bf16[32,32,128]{2,1,0:T(8,128)(2,1)} %bitcast.41), calls=%async_computation.3 | async-start | bytes 524288 | tf_op jit(solution)/shard_map/all_to_all | solution.py:107
Sparse Core Ops, SparseCore 0:
  80.6 44.5 all-gather.1
